TPU v7x, 32 devices: a whole 2x2x4 slice. The times are simulated.
32 devices in a mesh: grp: 2 (over y), fs: 4 (over z), tp: 4 (over x, core).
Axes of the slice: x: 2, y: 2, z: 4, core: 2. Of those that a mesh axis runs over, the one named last changes fastest.
Arguments:
- tokens: bfloat16 [2048, 2048], P(('grp', 'fs')), parts along dimension 0, may hold values from -6 to 6
- norm_gain: float32 [2048], P('fs'), may hold values from 0.1 to 1.9
- gate_master: float32 [4, 2048, 1024], P(None, 'fs', 'tp'), may hold values from -0.125 to 0.125
- up_master: float32 [4, 2048, 1024], P(None, 'fs', 'tp'), may hold values from -0.125 to 0.125
- chosen: int32 [2048, 2], P(('grp', 'fs')), parts along dimension 0, may hold values from 0 to 3, all different within a row; in each aligned block of 256 rows (0 to 255, 256 to 511, ...) at most 256 rows name the same one
- affinity: float32 [2048, 2], P(('grp', 'fs')), parts along dimension 0, may hold values from 0.05 to 1
Outputs:
- gate_served: bfloat16 [8, 2048, 1024], P(('grp', 'fs'), None, 'tp'), parts along dimension 0
- up_served: bfloat16 [8, 2048, 1024], P(('grp', 'fs'), None, 'tp'), parts along dimension 0
- hidden: bfloat16 [2048, 2, 1024], P(('grp', 'fs'), None, 'tp'), parts along dimension 0
There are 2 independent parts, one for each index of `grp`. A program takes and returns all parts, laid end to end along the dimension named above; an argument that names none is the same for every part. Nothing has to cross between parts.
Inputs may be any that keep to these rules, and one draw needn't show every extreme that they name: Among the rows of one index of fs (256 tokens, all their choices) no expert is chosen more than 256 times, a bound that some block reaches; the choices of one token differ.
All inputs are finite; a program needn't handle non-finite values.
Results may differ from a plain program's by a relative error of at most 0.023.
Values may be sent and summed in bfloat16 or wider, within the bound.
A program may use at most 64 MiB of HBM per device.

v0:
```python
import jax
import jax.numpy as jnp
from jax import lax
from jax.sharding import PartitionSpec as P


def on_device(tokens, norm_gain, gate_master, up_master, chosen, affinity):
    folded_gate = (gate_master * norm_gain[None, :, None]).astype(jnp.bfloat16)
    folded_up = (up_master * norm_gain[None, :, None]).astype(jnp.bfloat16)
    new_gate, new_up = (
        lax.all_to_all(folded_gate, "fs", split_axis=0, concat_axis=1, tiled=True),
        lax.all_to_all(folded_up, "fs", split_axis=0, concat_axis=1, tiled=True),
    )
    experts_all = gate_master.shape[0]
    tok_rows, width = tokens.shape
    top = chosen.shape[1]
    capacity = tok_rows * top * 2 // experts_all
    local = new_gate.shape[0]
    xfloat = tokens.astype(jnp.float32)
    scale = lax.rsqrt(jnp.mean(xfloat * xfloat, axis=-1) + 1e-06)
    share = affinity / jnp.sum(affinity, axis=-1, keepdims=True)
    flat_e = chosen.reshape(-1)
    onehot = (flat_e[:, None] == jnp.arange(experts_all, dtype=jnp.int32)[None, :]).astype(
        jnp.int32
    )
    slot = jnp.sum((jnp.cumsum(onehot, axis=0) - onehot) * onehot, axis=1)
    target = flat_e * capacity + slot
    owner = jnp.repeat(jnp.arange(tok_rows, dtype=jnp.int32), top)
    total = experts_all * capacity
    scale_buf = (
        jnp.zeros((total,), jnp.float32).at[target].set(scale[owner]).reshape(experts_all, capacity)
    )
    share_buf = (
        jnp.zeros((total,), jnp.float32)
        .at[target]
        .set(share.reshape(-1))
        .reshape(experts_all, capacity)
    )
    narrow = width // lax.axis_size("tp")
    own_cols = lax.dynamic_slice_in_dim(tokens, lax.axis_index("tp") * narrow, narrow, 1)
    row_buf = jnp.zeros((total, narrow), jnp.bfloat16).at[target].set(own_cols[owner])
    row_buf = row_buf.reshape(experts_all, capacity, narrow)
    got_rows, got_scale, got_share = (
        lax.all_to_all(row_buf, "fs", split_axis=0, concat_axis=0, tiled=True),
        lax.all_to_all(
            scale_buf.astype(jnp.bfloat16), "fs", split_axis=0, concat_axis=0, tiled=True
        ).astype(scale_buf.dtype),
        lax.all_to_all(
            share_buf.astype(jnp.bfloat16), "fs", split_axis=0, concat_axis=0, tiled=True
        ).astype(share_buf.dtype),
    )
    sources = got_rows.shape[0] // local
    got_rows = got_rows.reshape(sources, local, capacity, narrow)
    piece = lax.all_gather(got_rows, "tp", axis=3, tiled=True)
    more_gate = jnp.einsum("secd,edf->secf", piece, new_gate, preferred_element_type=jnp.float32)
    more_up = jnp.einsum("secd,edf->secf", piece, new_up, preferred_element_type=jnp.float32)
    gate = more_gate
    up = more_up
    factor = got_scale.reshape(sources, local, capacity)[..., None]
    weight = got_share.reshape(sources, local, capacity)[..., None]
    gate = gate * factor
    up = up * factor
    hidden_rows = (weight * jax.nn.silu(gate) * up).astype(jnp.bfloat16)
    hidden_rows = hidden_rows.reshape(sources * local, capacity, hidden_rows.shape[3])
    back = lax.all_to_all(hidden_rows, "fs", split_axis=0, concat_axis=0, tiled=True)
    picked = back.reshape(total, back.shape[2])[target].reshape(tok_rows, top, back.shape[2])
    return (new_gate, new_up, picked)


def solution(mesh):
    return jax.shard_map(
        on_device,
        mesh=mesh,
        in_specs=(
            P(("grp", "fs"), None),
            P("fs"),
            P(None, "fs", "tp"),
            P(None, "fs", "tp"),
            P(("grp", "fs"), None),
            P(("grp", "fs"), None),
        ),
        out_specs=(
            P(("grp", "fs"), None, "tp"),
            P(("grp", "fs"), None, "tp"),
            P(("grp", "fs"), None, "tp"),
        ),
        check_vma=False,
    )
```

profile of v0, /device:TPU:0, one launch (start us, length us, event | category | flops | bytes accessed | tf_op | source)
XLA Modules:
  0.0 163.8 jit_solution(18356809726918053598)
XLA Ops:
  7.2 0.0 all-gather.3.cloned.1.call-start
  7.2 0.7 broadcast_multiply_fusion
  7.9 0.8 copy.26
  8.7 0.1 eq.29
  8.9 0.1 eq.25
  9.0 0.1 copy.25
  9.1 0.1 mul.75
  9.3 1.2 reduce-window.6
  10.5 0.2 slice_reduce_fusion
  10.8 0.2 reduce-window.9
  10.9 0.1 add_bitcast_fusion
  11.0 0.1 reshape.174
  11.2 1.0 constant_dynamic-slice_fusion
  12.2 0.0 copy-start.1
  12.2 0.0 copy-start
  12.2 5.0 %scatter_custom_fusion.1 = bf16[1024,512]{1,0:T(8,128)(2,1)S(1)} fusion(s32[512]{0:T(512)S(1)} %bitcast.83, bf16[256,512]{1,0:T(8,128)(2,1)S(1)} %constant_dynamic-slice_fusion, s32[1024]{0:T(1024)S(1)} %pad_clamp_fusion.1, bf16[]{:T(256)} %constant.15.clone.1), kind=kCustom, calls=%fused_computation.18 | custom fusion | bytes 1048578 | tf_op jit(solution)/shard_map/scatter | solution.py:41
  17.3 32.0 %all_to_all.46 = bf16[4,256,512]{2,1,0:T(8,128)(2,1)} all-to-all(bf16[4,256,512]{2,1,0:T(8,128)(2,1)S(1)} %bitcast.82), channel_id=1, replica_groups=mesh['grp'=2,'fs'=4,'tp'=4] {'fs'}, dimensions={0} | all-to-all | bytes 2097152 | tf_op jit(solution)/shard_map/all_to_all | solution.py:44
  49.3 0.0 copy-start.2
  49.3 0.0 all-gather.3.cloned.1.call-update
  49.3 0.0 copy-done.1
  49.3 0.1 copy.28
  49.5 0.1 reshape.212
  49.6 2.4 %scatter_custom_fusion = f32[1024]{0:T(1024)S(1)} fusion(s32[512]{0:T(512)S(1)} %bitcast.84, f32[512]{0:T(512)S(1)} %reshape.212, f32[]{:T(128)} %constant.11.clone.1), kind=kCustom, calls=%fused_computation.38 | custom fusion | bytes 4100 | tf_op jit(solution)/shard_map/scatter | solution.py:36
  52.1 0.5 broadcast.103
  52.6 0.7 reduce.3
  53.3 0.6 reshape.249
  53.9 3.2 %all-to-all-start.2 = ((bf16[4,2,128]{2,1,0:T(2,128)(2,1)}), bf16[4,2,128]{2,1,0:T(2,128)(2,1)S(1)}, u32[]{:S(2)}, u32[]{:S(2)}) async-start(bf16[4,2,128]{2,1,0:T(2,128)(2,1)} %reshape.249), calls=%async_computation.2 | async-start | bytes 4096 | tf_op jit(solution)/shard_map/all_to_all | solution.py:48
  57.1 0.0 copy-done
  57.1 0.3 multiply_reduce_fusion
  57.4 3.5 %gather_fusion = f32[512]{0:T(512)S(1)} fusion(f32[256]{0:T(256)S(1)} %add_rsqrt_fusion, s32[1024]{0:T(1024)S(1)} %pad_clamp_fusion.1), kind=kCustom, calls=%fused_computation.1 | custom fusion | bytes 6144 | tf_op jit(solution)/shard_map/gather | solution.py:31
  61.0 2.4 %scatter_custom_fusion.2 = f32[1024]{0:T(1024)S(1)} fusion(s32[512]{0:T(512)S(1)} %bitcast.85, f32[512]{0:T(512)S(1)} %gather_fusion, f32[]{:T(128)} %constant.11.clone.1), kind=kCustom, calls=%fused_computation.36 | custom fusion | bytes 4100 | tf_op jit(solution)/shard_map/scatter | solution.py:31
  63.4 0.7 reduce.2
  64.1 0.6 reshape.247
  64.7 0.0 all-to-all-done.2
  64.7 5.0 %all-to-all-start.4 = ((bf16[4,2,128]{2,1,0:T(2,128)(2,1)}), bf16[4,2,128]{2,1,0:T(2,128)(2,1)S(1)}, u32[]{:S(2)}, u32[]{:S(2)}) async-start(bf16[4,2,128]{2,1,0:T(2,128)(2,1)} %reshape.247), calls=%async_computation.4 | async-start | bytes 4096 | tf_op jit(solution)/shard_map/all_to_all | solution.py:45
  69.7 0.0 copy-done.2
  69.7 3.5 %multiply_convert_fusion = (bf16[4,512,256]{2,1,0:T(8,128)(2,1)}, bf16[4,512,256]{2,1,0:T(8,128)(2,1)S(1)}) fusion(f32[4,512,256]{2,1,0:T(8,128)} %param.9, f32[512]{0:T(512)S(1)} %copy-done.2, f32[4,512,256]{2,1,0:T(8,128)} %param.8), kind=kLoop, calls=%fused_computation.7 | loop fusion | flops 2097152 | bytes 6293504 | tf_op jit(solution)/shard_map/convert_element_type | solution.py:9
  73.3 2.0 %all-to-all-done.4 = bf16[4,2,128]{2,1,0:T(2,128)(2,1)S(1)} async-done(((bf16[4,2,128]{2,1,0:T(2,128)(2,1)}), bf16[4,2,128]{2,1,0:T(2,128)(2,1)S(1)}, u32[]{:S(2)}, u32[]{:S(2)}) %all-to-all-start.4) | async-done | bytes 2080 | tf_op jit(solution)/shard_map/all_to_all | solution.py:45
  75.2 26.7 %all_to_all.47 = bf16[4,512,256]{2,1,0:T(8,128)(2,1)S(1)} all-to-all(bf16[4,512,256]{2,1,0:T(8,128)(2,1)S(1)} %get-tuple-element.4), channel_id=1, replica_groups=mesh['grp'=2,'fs'=4,'tp'=4] {'fs'}, dimensions={0} | all-to-all | bytes 2097152 | tf_op jit(solution)/shard_map/all_to_all | solution.py:11
  101.9 3.7 %all-to-all-start.1 = ((bf16[4,512,256]{2,1,0:T(8,128)(2,1)}), bf16[4,512,256]{2,1,0:T(8,128)(2,1)S(1)}, u32[]{:S(2)}, u32[]{:S(2)}) async-start(bf16[4,512,256]{2,1,0:T(8,128)(2,1)} %get-tuple-element.3), calls=%async_computation.1 | async-start | bytes 2097152 | tf_op jit(solution)/shard_map/all_to_all | solution.py:12
  105.7 0.0 all-gather.3.cloned.1.call-done
  105.7 3.5 %fusion.3 = f32[4,1,256,256]{2,3,0,1:T(8,128)S(1)} fusion(bf16[2048,256,1]{1,0,2:T(8,128)(2,1)S(1)} %bitcast.78, bf16[4,256,2048]{2,1,0:T(8,128)(2,1)} %all-gather.3.cloned.1.call-done, f32[4,256]{1,0:T(4,128)S(1)} %bitcast.91), kind=kOutput, calls=%fused_computation.14 | convolution fusion | flops 1074003968 | bytes 6295552 | tf_op jit(solution)/shard_map/secd,edf->secf/dot_general | solution.py:55
  109.2 20.8 %all-to-all-done.1 = bf16[4,512,256]{2,1,0:T(8,128)(2,1)S(1)} async-done(((bf16[4,512,256]{2,1,0:T(8,128)(2,1)}), bf16[4,512,256]{2,1,0:T(8,128)(2,1)S(1)}, u32[]{:S(2)}, u32[]{:S(2)}) %all-to-all-start.1) | async-done | bytes 1048608 | tf_op jit(solution)/shard_map/all_to_all | solution.py:12
  130.1 4.5 %fusion.6 = bf16[4,256,256]{1,2,0:T(8,128)(2,1)} fusion(bf16[2048,256,1]{1,0,2:T(8,128)(2,1)S(1)} %bitcast.80, bf16[4,256,2048]{2,1,0:T(8,128)(2,1)} %all-gather.3.cloned.1.call-done, f32[4,1,256,256]{2,3,0,1:T(8,128)S(1)} %fusion.3, f32[4,256]{1,0:T(4,128)S(1)} %bitcast.92, f32[4,256]{1,0:T(4,128)S(1)} %bitcast.90), kind=kOutput, calls=%fused_computation.17 | convolution fusion | flops 1075838976 | bytes 6823936 | tf_op jit(solution)/shard_map/secd,edf->secf/dot_general | solution.py:56
  134.6 3.5 %all-to-all-start.5 = ((bf16[4,256,256]{1,2,0:T(8,128)(2,1)}), bf16[4,256,256]{1,2,0:T(8,128)(2,1)S(1)}, u32[]{:S(2)}, u32[]{:S(2)}) async-start(bf16[4,256,256]{1,2,0:T(8,128)(2,1)} %fusion.6), calls=%async_computation.5 | async-start | bytes 1048576 | tf_op jit(solution)/shard_map/all_to_all | solution.py:65
  138.1 14.0 %all-to-all-done.5 = bf16[4,256,256]{1,2,0:T(8,128)(2,1)S(1)} async-done(((bf16[4,256,256]{1,2,0:T(8,128)(2,1)}), bf16[4,256,256]{1,2,0:T(8,128)(2,1)S(1)}, u32[]{:S(2)}, u32[]{:S(2)}) %all-to-all-start.5) | async-done | bytes 524320 | tf_op jit(solution)/shard_map/all_to_all | solution.py:65
  152.1 0.2 copy.33
  152.3 2.0 %gather_fusion.1 = bf16[512,256]{1,0:T(8,128)(2,1)S(1)} fusion(bf16[1024,256]{1,0:T(8,128)(2,1)S(1)} %bitcast.77, s32[1024]{0:T(1024)S(1)} %pad_clamp_fusion), kind=kCustom, calls=%fused_computation.2 | custom fusion | bytes 526336 | tf_op jit(solution)/shard_map/gather | solution.py:66
  154.2 0.8 reshape.181
  155.0 1.0 copy.46
  156.0 1.0 copy.47
  (18 shorter events, 0.2 us)
Async XLA Ops:
  7.2 98.6 %all-gather.3.cloned.1.call-start = ((), (), s32[]{:S(2)}) async-start(), calls=%async_computation.6 | async-start | bytes 5242880 | tf_op jit(solution)/shard_map/all_gather | solution.py:54
  12.2 37.1 %copy-start.1 = (f32[256,2]{0,1:T(2,128)S(1)}, f32[256,2]{0,1:T(2,128)}, u32[]{:S(2)}) copy-start(f32[256,2]{0,1:T(2,128)} %param.11) | copy-start | bytes 6148
  12.2 44.9 %copy-start = (bf16[256,2048]{1,0:T(8,128)(2,1)S(1)}, bf16[256,2048]{1,0:T(8,128)(2,1)}, u32[]{:S(2)}) copy-start(bf16[256,2048]{1,0:T(8,128)(2,1)} %param.6) | copy-start | bytes 3145732
  49.3 20.5 %copy-start.2 = (f32[512]{0:T(512)S(1)}, f32[512]{0:T(512)}, u32[]{:S(2)}) copy-start(f32[512]{0:T(512)} %param.7) | copy-start | bytes 6148
  53.9 10.8 %all-to-all-start.2 = ((bf16[4,2,128]{2,1,0:T(2,128)(2,1)}), bf16[4,2,128]{2,1,0:T(2,128)(2,1)S(1)}, u32[]{:S(2)}, u32[]{:S(2)}) async-start(bf16[4,2,128]{2,1,0:T(2,128)(2,1)} %reshape.249), calls=%async_computation.2 | async-start | bytes 4096 | tf_op jit(solution)/shard_map/all_to_all | solution.py:48
  64.7 10.5 %all-to-all-start.4 = ((bf16[4,2,128]{2,1,0:T(2,128)(2,1)}), bf16[4,2,128]{2,1,0:T(2,128)(2,1)S(1)}, u32[]{:S(2)}, u32[]{:S(2)}) async-start(bf16[4,2,128]{2,1,0:T(2,128)(2,1)} %reshape.247), calls=%async_computation.4 | async-start | bytes 4096 | tf_op jit(solution)/shard_map/all_to_all | solution.py:45
  101.9 28.1 %all-to-all-start.1 = ((bf16[4,512,256]{2,1,0:T(8,128)(2,1)}), bf16[4,512,256]{2,1,0:T(8,128)(2,1)S(1)}, u32[]{:S(2)}, u32[]{:S(2)}) async-start(bf16[4,512,256]{2,1,0:T(8,128)(2,1)} %get-tuple-element.3), calls=%async_computation.1 | async-start | bytes 2097152 | tf_op jit(solution)/shard_map/all_to_all | solution.py:12
  134.6 17.5 %all-to-all-start.5 = ((bf16[4,256,256]{1,2,0:T(8,128)(2,1)}), bf16[4,256,256]{1,2,0:T(8,128)(2,1)S(1)}, u32[]{:S(2)}, u32[]{:S(2)}) async-start(bf16[4,256,256]{1,2,0:T(8,128)(2,1)} %fusion.6), calls=%async_computation.5 | async-start | bytes 1048576 | tf_op jit(solution)/shard_map/all_to_all | solution.py:65
Sparse Core Ops, SparseCore 0:
  49.4 33.5 all-gather.2
where the time goes:
time: 164 us
  blocking collectives  58.7 us (36%)
  waiting for transfers between devices  36.8 us (22%)
  local copies, waits for them, and re-layouts  23.1 us (14%)
  starting transfers between devices  15.5 us (9%)
  between operations  14.3 us (9%)
  matrix products  7.99 us (5%)
  other arithmetic  7.42 us (5%)
    all_to_all x1, blocking collectives, on_device(): lax.all_to_all(row_buf, 'fs', split_axis=0, concat_axis=0, tiled=True)  32 us
    all_to_all x1, blocking collectives, on_device(): lax.all_to_all(folded_gate, 'fs', split_axis=0, concat_axis=1, tiled=True)  26.7 us
    all_to_all x1, waiting for transfers between devices, on_device(): lax.all_to_all(folded_up, 'fs', split_axis=0, concat_axis=1, tiled=True)  20.8 us
    all_to_all x1, waiting for transfers between devices, on_device(): lax.all_to_all(hidden_rows, 'fs', split_axis=0, concat_axis=0, tiled=True)  14 us
    all_to_all x1, starting transfers between devices, on_device(): lax.all_to_all(scale_buf.astype(jnp.bfloat16), 'fs', split_axis=0, concat...  5.05 us
    scatter x1, local copies, waits for them, and re-layouts, on_device(): jnp.zeros((total, narrow), jnp.bfloat16).at[target].set(own_cols[owner])  5.05 us
    dot_general x1, matrix products, on_device(): jnp.einsum('secd,edf->secf', piece, new_up, preferred_element_type=jnp.fl...  4.48 us
    unnamed x15, local copies, waits for them, and re-layouts  3.97 us
  transfers between devices with their start and end apart: 5, of which 3 were waited for; matrix products, arithmetic and copies ran while one was open for 12% of the time, Pallas kernels for 0%

commit v1 on v0

--- a/solution.py
+++ b/solution.py
@@ -1,10 +1,17 @@
+import functools
+
 import jax
 import jax.numpy as jnp
 from jax import lax
+from jax.experimental import pallas as pl
+from jax.experimental.pallas import tpu as pltpu
 from jax.sharding import PartitionSpec as P
 
-
-def on_device(tokens, norm_gain, gate_master, up_master, chosen, affinity):
+MESH = pl.DeviceIdType.MESH
+CHUNKS = 2
+
+
+def routed(tokens, norm_gain, gate_master, up_master, chosen, affinity):
     folded_gate = (gate_master * norm_gain[None, :, None]).astype(jnp.bfloat16)
     folded_up = (up_master * norm_gain[None, :, None]).astype(jnp.bfloat16)
     new_gate, new_up = (
@@ -52,10 +59,8 @@
     sources = got_rows.shape[0] // local
     got_rows = got_rows.reshape(sources, local, capacity, narrow)
     piece = lax.all_gather(got_rows, "tp", axis=3, tiled=True)
-    more_gate = jnp.einsum("secd,edf->secf", piece, new_gate, preferred_element_type=jnp.float32)
-    more_up = jnp.einsum("secd,edf->secf", piece, new_up, preferred_element_type=jnp.float32)
-    gate = more_gate
-    up = more_up
+    gate = jnp.einsum("secd,edf->secf", piece, new_gate, preferred_element_type=jnp.float32)
+    up = jnp.einsum("secd,edf->secf", piece, new_up, preferred_element_type=jnp.float32)
     factor = got_scale.reshape(sources, local, capacity)[..., None]
     weight = got_share.reshape(sources, local, capacity)[..., None]
     gate = gate * factor
@@ -65,6 +70,325 @@
     back = lax.all_to_all(hidden_rows, "fs", split_axis=0, concat_axis=0, tiled=True)
     picked = back.reshape(total, back.shape[2])[target].reshape(tok_rows, top, back.shape[2])
     return (new_gate, new_up, picked)
+
+
+def dense_kernel(
+    n, nt, width,
+    tok_hbm, gain_ref, gate_hbm, up_hbm, chosen_ref, aff_ref,
+    gate_out, up_out, hid_out,
+    tok, wf, own, wsend, W, scale, hs, hr,
+    ls_tok, ls_w, ls_own, os,
+    ss_tz, ss_tx, ss_tm, rs_tok, ss_w, rs_w, ss_y, ss_h, rs_h,
+):
+    g, z, t = lax.axis_index("grp"), lax.axis_index("fs"), lax.axis_index("tp")
+    depth, fcols = wf.shape[1], wf.shape[2]
+    fc = fcols // CHUNKS
+    mate = t + 1 - 2 * lax.rem(t, 2)
+    xq = lax.rem(t + 2, nt)
+    xmate = lax.rem(mate + 2, nt)
+    rows = tok.shape[2]
+
+    def remote(src, dst, ssem, rsem, **dev):
+        return pltpu.make_async_remote_copy(
+            src_ref=src, dst_ref=dst, send_sem=ssem, recv_sem=rsem, device_id=dev, device_id_type=MESH
+        )
+
+    def tok_load(q):
+        return pltpu.make_async_copy(
+            tok_hbm.at[:, pl.ds(pl.multiple_of(q * depth, depth), depth)], tok.at[z, q], ls_tok.at[q]
+        )
+
+    tok_load(t).start()
+    for off in range(1, n):
+        e = lax.rem(z + off, n)
+
+        @pl.when(g == 0)
+        def _():
+            pltpu.make_async_copy(gate_hbm.at[e], wf.at[e], ls_w.at[e]).start()
+
+        @pl.when(g != 0)
+        def _():
+            pltpu.make_async_copy(up_hbm.at[e], wf.at[e], ls_w.at[e]).start()
+
+    own_loads = [
+        pltpu.make_async_copy(gate_hbm.at[z], own.at[0], ls_own.at[0]),
+        pltpu.make_async_copy(up_hbm.at[z], own.at[1], ls_own.at[1]),
+    ]
+    for copy in own_loads:
+        copy.start()
+    for off in range(1, nt):
+        tok_load(lax.rem(t + off, nt)).start()
+
+    barrier = pltpu.get_barrier_semaphore()
+    for off in range(1, n):
+        pl.semaphore_signal(barrier, 1, device_id={"fs": lax.rem(z + off, n)}, device_id_type=MESH)
+    pl.semaphore_signal(barrier, 1, device_id={"grp": 1 - g}, device_id_type=MESH)
+    pl.semaphore_signal(barrier, 1, device_id={"tp": mate}, device_id_type=MESH)
+    pl.semaphore_signal(barrier, 1, device_id={"tp": xq}, device_id_type=MESH)
+    pl.semaphore_wait(barrier, n + 2)
+
+    def tz(s, step):
+        return remote(tok.at[s, t], tok.at[s, t], ss_tz.at[s, (step + 1) // 2], rs_tok.at[s, t], fs=z + step)
+
+    def tx(s):
+        return remote(tok.at[s, t], tok.at[s, t], ss_tx.at[s], rs_tok.at[s, t], tp=xq)
+
+    def tm(s, q, i):
+        return remote(tok.at[s, q], tok.at[s, q], ss_tm.at[s, i], rs_tok.at[s, q], tp=mate)
+
+    def tok_wait(s, q):
+        remote(tok.at[s, q], tok.at[s, q], ss_tx.at[s], rs_tok.at[s, q], tp=mate).wait_recv()
+
+    def sides(d, fn):
+        for sign in (1, -1):
+            s = z + sign * d
+
+            @pl.when((s >= 0) & (s < n))
+            def _():
+                fn(s, sign)
+
+    tok_load(t).wait()
+    sides(1, lambda s, sign: tz(z, sign).start())
+
+    gcol = jnp.transpose(jnp.broadcast_to(gain_ref[...], (128, depth)))
+    gcol = jnp.concatenate([gcol] * (fc // 128), axis=1) if fc > 128 else gcol
+
+    def fold(s, sign):
+        pltpu.make_async_copy(gate_hbm.at[s], wf.at[s], ls_w.at[s]).wait()
+        for c in range(CHUNKS):
+            wsend[s, c] = (wf[s, :, c * fc : (c + 1) * fc] * gcol).astype(jnp.bfloat16)
+
+    def lanes(m):
+        return pl.ds(pl.multiple_of(m * fc, fc), fc)
+
+    def wcopy(c, to):
+        return remote(wsend.at[to, c], W.at[z, c, :, lanes(g)], ss_w.at[c, to], rs_w.at[g, c, z], fs=to)
+
+    def send_weights(c):
+        for d in range(n - 1, 0, -1):
+            sides(d, lambda s, sign: wcopy(c, s).start())
+
+    for d in range(n - 1, 0, -1):
+        sides(d, fold)
+    send_weights(0)
+
+    def out_copy(m, c, s):
+        ref = (gate_out, up_out)[m]
+        return pltpu.make_async_copy(
+            W.at[s, c, :, pl.ds(m * fc, fc)],
+            ref.at[0, pl.ds(pl.multiple_of(s * depth, depth), depth), pl.ds(c * fc, fc)],
+            os.at[m, c, s],
+        )
+
+    for m in range(2):
+        own_loads[m].wait()
+        for c in range(CHUNKS):
+            W[z, c, :, m * fc : (m + 1) * fc] = (own[m, :, c * fc : (c + 1) * fc] * gcol).astype(jnp.bfloat16)
+
+    def arrive(s, sign):
+        tok_wait(s, t)
+        nxt = z - sign
+
+        @pl.when((nxt >= 0) & (nxt < n))
+        def _():
+            tz(s, -sign).start()
+
+        tx(s).start()
+        tm(s, t, 0).start()
+
+    def xrelay(s, sign):
+        tok_wait(s, xq)
+        tm(s, xq, 1).start()
+
+    def ycopy(c, s):
+        return remote(W.at[s, c, :, lanes(g)], W.at[s, c, :, lanes(g)], ss_y.at[c, s], rs_w.at[g, c, s], grp=1 - g)
+
+    def yforward(c):
+        def one(s, sign):
+            remote(wsend.at[s, c], W.at[s, c, :, lanes(g)], ss_w.at[c, s], rs_w.at[g, c, s], fs=s).wait_recv()
+            ycopy(c, s).start()
+
+        for d in range(1, n):
+            sides(d, one)
+
+    def ywait(c):
+        def one(s, sign):
+            o = 1 - g
+            remote(W.at[s, c, :, lanes(o)], W.at[s, c, :, lanes(o)], ss_y.at[c, s], rs_w.at[o, c, s], grp=o).wait_recv()
+
+        for d in range(1, n):
+            sides(d, one)
+        for s in range(n):
+            for m in range(2):
+                out_copy(m, c, s).start()
+
+    def hcopy(c, to):
+        return remote(hs.at[to, c], hr.at[z, c], ss_h.at[c, to], rs_h.at[c, z], fs=to)
+
+    def sumsq(s):
+        total = jnp.zeros((rows, 1), jnp.float32)
+        for q in range(nt):
+            x = tok[s, q].astype(jnp.float32)
+            total = total + jnp.sum(x * x, axis=-1, keepdims=True)
+        scale[s] = jnp.broadcast_to(lax.rsqrt(total / width + 1e-06), (rows, fc))
+
+    def compute(c):
+        def body(i, carry):
+            s = lax.rem(z + 1 + i, n)
+            acc = jnp.dot(tok[s, 0], W[0, c], preferred_element_type=jnp.float32)
+            for q in range(1, nt):
+                acc = acc + jnp.dot(tok[s, q], W[q, c], preferred_element_type=jnp.float32)
+            gate = acc[:, :fc] * scale[s]
+            up = acc[:, fc:] * scale[s]
+            h = (gate / (1.0 + jnp.exp(-gate)) * up).astype(jnp.bfloat16)
+
+            @pl.when(s != z)
+            def _():
+                hs[s, c] = h
+                hcopy(c, s).start()
+
+            @pl.when(s == z)
+            def _():
+                hr[z, c] = h
+
+            return carry
+
+        lax.fori_loop(0, n, body, 0)
+
+    sides(1, arrive)
+    sides(2, arrive)
+    for c in range(1, CHUNKS):
+        send_weights(c)
+    sides(1, xrelay)
+    yforward(0)
+    for d in range(3, n):
+        sides(d, arrive)
+    for d in range(2, n):
+        sides(d, xrelay)
+    for off in range(1, nt):
+        tok_load(lax.rem(t + off, nt)).wait()
+    sumsq(z)
+
+    def rest(s, sign):
+        tok_wait(s, mate)
+        tok_wait(s, xmate)
+        sumsq(s)
+
+    for d in range(1, n):
+        sides(d, rest)
+    ywait(0)
+    compute(0)
+    for c in range(1, CHUNKS):
+        yforward(c)
+        ywait(c)
+        compute(c)
+
+    aff = aff_ref[...]
+    share = aff / jnp.sum(aff, axis=-1, keepdims=True)
+    top = aff.shape[1]
+    for c in range(CHUNKS):
+        for off in range(1, n):
+            s = lax.rem(z + off, n)
+            remote(hs.at[s, c], hr.at[s, c], ss_h.at[c, s], rs_h.at[c, s], fs=s).wait_recv()
+        for k in range(top):
+            ch = jnp.broadcast_to(chosen_ref[:, k : k + 1], (rows, fc))
+            picked = jnp.zeros((rows, fc), jnp.float32)
+            for e in range(n):
+                picked = jnp.where(ch == e, hr[e, c].astype(jnp.float32), picked)
+            hid_out[:, k * fcols + c * fc : k * fcols + (c + 1) * fc] = (
+                picked * share[:, k : k + 1]
+            ).astype(jnp.bfloat16)
+
+    sides(1, lambda s, sign: tz(z, sign).wait_send())
+
+    def drain(s, sign):
+        nxt = z - sign
+
+        @pl.when((nxt >= 0) & (nxt < n))
+        def _():
+            tz(s, -sign).wait_send()
+
+        tx(s).wait_send()
+        tm(s, t, 0).wait_send()
+        tm(s, xq, 1).wait_send()
+        for c in range(CHUNKS):
+            wcopy(c, s).wait_send()
+            ycopy(c, s).wait_send()
+            hcopy(c, s).wait_send()
+
+    for d in range(1, n):
+        sides(d, drain)
+    for c in range(CHUNKS):
+        for s in range(n):
+            for m in range(2):
+                out_copy(m, c, s).wait()
+
+
+def dense(tokens, norm_gain, gate_master, up_master, chosen, affinity):
+    n, nt = lax.axis_size("fs"), lax.axis_size("tp")
+    rows, width = tokens.shape
+    experts, depth, fcols = gate_master.shape
+    top = chosen.shape[1]
+    fc = fcols // CHUNKS
+    bf, f32 = jnp.bfloat16, jnp.float32
+    dma = pltpu.SemaphoreType.DMA
+    any_spec = pl.BlockSpec(memory_space=pl.ANY)
+    vmem = pl.BlockSpec(memory_space=pltpu.VMEM)
+    gate, up, hid = pl.pallas_call(
+        functools.partial(dense_kernel, n, nt, width),
+        out_shape=(
+            jax.ShapeDtypeStruct((1, width, fcols), bf),
+            jax.ShapeDtypeStruct((1, width, fcols), bf),
+            jax.ShapeDtypeStruct((rows, top * fcols), bf),
+        ),
+        in_specs=[any_spec, vmem, any_spec, any_spec, vmem, vmem],
+        out_specs=(any_spec, any_spec, vmem),
+        scratch_shapes=[
+            pltpu.VMEM((n, nt, rows, depth), bf),
+            pltpu.VMEM((n, depth, fcols), f32),
+            pltpu.VMEM((2, depth, fcols), f32),
+            pltpu.VMEM((n, CHUNKS, depth, fc), bf),
+            pltpu.VMEM((n, CHUNKS, depth, 2 * fc), bf),
+            pltpu.VMEM((n, rows, fc), f32),
+            pltpu.VMEM((n, CHUNKS, rows, fc), bf),
+            pltpu.VMEM((n, CHUNKS, rows, fc), bf),
+            dma((nt,)),
+            dma((n,)),
+            dma((2,)),
+            dma((2, CHUNKS, n)),
+            dma((n, 2)),
+            dma((n,)),
+            dma((n, 2)),
+            dma((n, nt)),
+            dma((CHUNKS, n)),
+            dma((2, CHUNKS, n)),
+            dma((CHUNKS, n)),
+            dma((CHUNKS, n)),
+            dma((CHUNKS, n)),
+        ],
+        compiler_params=pltpu.CompilerParams(
+            collective_id=0, has_side_effects=True, vmem_limit_bytes=48 * 1024 * 1024
+        ),
+    )(tokens, norm_gain.reshape(1, depth), gate_master, up_master, chosen, affinity)
+    return gate, up, hid.reshape(rows, top, fcols)
+
+
+def on_device(tokens, norm_gain, gate_master, up_master, chosen, affinity):
+    n, nt = lax.axis_size("fs"), lax.axis_size("tp")
+    experts, depth, fcols = gate_master.shape
+    rows, width = tokens.shape
+    capacity = rows * chosen.shape[1] * 2 // experts
+    fits = (
+        experts == n
+        and capacity >= rows
+        and n >= 3
+        and nt == 4
+        and lax.axis_size("grp") == 2
+        and width == nt * depth
+        and fcols % (CHUNKS * 128) == 0
+    )
+    run = dense if fits else routed
+    return run(tokens, norm_gain, gate_master, up_master, chosen, affinity)
 
 
 def solution(mesh):

time: 164 us -> 79.6 us (0.49)
  Pallas kernels: 0 us -> 70.9 us
  blocking collectives: 58.7 us -> 0 us
  waiting for transfers between devices: 36.8 us -> 0 us
  starting transfers between devices: 15.5 us -> 0 us
  local copies, waits for them, and re-layouts: 23.1 us -> 7.82 us
  between operations: 14.3 us -> 0.67 us
  matrix products: 7.99 us -> 0 us
  other arithmetic: 7.42 us -> 0 us
    pallas_call x0 -> x1, Pallas kernels: none -> 70.9 us  [dense(): pl.pallas_call(functools.partial(dense_kernel, n, nt, width), out_shape=(...]
    all_to_all x2 -> x0, blocking collectives: 58.7 us -> none  [the longest x1 32 us: on_device(): lax.all_to_all(row_buf, 'fs', split_axis=0, concat_axis=0, tiled=True)]
    all_to_all x4 -> x0, waiting for transfers between devices: 36.8 us -> none  [the longest x1 20.8 us: on_device(): lax.all_to_all(folded_up, 'fs', split_axis=0, concat_axis=1, tiled=True)]
    all_to_all x4 -> x0, starting transfers between devices: 15.4 us -> none  [the longest x1 5.05 us: on_device(): lax.all_to_all(scale_buf.astype(jnp.bfloat16), 'fs', split_axis=0, concat...]
    scatter x3 -> x0, local copies, waits for them, and re-layouts: 9.94 us -> none  [the longest x1 5.05 us: on_device(): jnp.zeros((total, narrow), jnp.bfloat16).at[target].set(own_cols[owner])]
    dot_general x2 -> x0, matrix products: 7.99 us -> none  [the longest x1 4.48 us: on_device(): jnp.einsum('secd,edf->secf', piece, new_up, preferred_element_type=jnp.fl...]
    gather x2 -> x0, local copies, waits for them, and re-layouts: 5.47 us -> none  [the longest x1 3.52 us: on_device(): scale[owner]]
    convert_element_type x6 -> x0, other arithmetic: 4.88 us -> none  [the longest x1 3.54 us: on_device(): folded_up = (up_master * norm_gain[None, :, None]).astype(jnp.bfloat16)]
  transfers between devices with their start and end apart: 5 -> 0, of which waited for: 3 -> 0; matrix products, arithmetic and copies ran while one was open for 12% -> 0% of each run, Pallas kernels for 0% -> 0%
where the time goes in v1:
time: 79.6 us; the launch traced here: 79.4 us
  Pallas kernels  70.9 us (89%)
  local copies, waits for them, and re-layouts  7.82 us (10%)
    pallas_call x1, Pallas kernels, dense(): pl.pallas_call(functools.partial(dense_kernel, n, nt, width), out_shape=(...  70.9 us
    unnamed x10, local copies, waits for them, and re-layouts  7.06 us

profile of v1, /device:TPU:0, one launch (start us, length us, event | category | flops | bytes accessed | tf_op | source)
XLA Modules:
  0.0 79.4 jit_solution(12170037331647727575)
XLA Ops:
  0.6 0.8 %copy.9.chosen_ref = s32[256,2]{1,0:T(8,128)S(1)} copy(s32[256,2]{0,1:T(2,128)} %param.10) | data formatting | bytes 4096 | tf_op args[4]
  1.4 0.8 %copy.10.aff_ref = f32[256,2]{1,0:T(8,128)S(1)} copy(f32[256,2]{0,1:T(2,128)} %param.11) | data formatting | bytes 4096 | tf_op args[5]
  2.3 0.0 copy-start
  2.3 1.6 %copy-done = f32[4,512,256]{2,1,0:T(8,128)S(1)} copy-done((f32[4,512,256]{2,1,0:T(8,128)S(1)}, f32[4,512,256]{2,1,0:T(8,128)}, u32[]{:S(2)}) %copy-start) | copy-done | bytes 2097176
  3.9 0.0 copy-start.1
  3.9 1.2 %copy-done.1 = bf16[256,2048]{1,0:T(8,128)(2,1)S(1)} copy-done((bf16[256,2048]{1,0:T(8,128)(2,1)S(1)}, bf16[256,2048]{1,0:T(8,128)(2,1)}, u32[]{:S(2)}) %copy-start.1) | copy-done | bytes 1048600
  5.1 0.0 copy-start.2
  5.1 0.7 copy-done.2
  5.8 70.9 %shard_map.85 = (bf16[1,2048,256]{2,1,0:T(8,128)(2,1)S(1)}, bf16[1,2048,256]{2,1,0:T(8,128)(2,1)S(1)}, bf16[256,512]{1,0:T(8,128)(2,1)S(1)}) custom-call(bf16[256,2048]{1,0:T(8,128)(2,1)S(1)} %copy-done.1, f32[1,512]{1,0:T(1,128)S(1)} %bitcast.1, f32[4,512,256]{2,1,0:T(8,128)S(1)} %copy-done, f32[4,512,256]{2,1,0:T(8,128)} %up_hbm.1, ...), custom_call_target="tpu_custom_call" | custom-call | tf_op jit(solution)/shard_map/pallas_call | solution.py:337
  76.7 0.8 reshape.13
  77.4 1.0 %copy.13 = bf16[1,2048,256]{2,1,0:T(8,128)(2,1)} copy(bf16[1,2048,256]{2,1,0:T(8,128)(2,1)S(1)} %get-tuple-element.12) | data formatting | bytes 2097152
  78.4 1.0 %copy.14 = bf16[1,2048,256]{2,1,0:T(8,128)(2,1)} copy(bf16[1,2048,256]{2,1,0:T(8,128)(2,1)S(1)} %get-tuple-element.13) | data formatting | bytes 2097152
Async XLA Ops:
  2.3 1.6 %copy-start = (f32[4,512,256]{2,1,0:T(8,128)S(1)}, f32[4,512,256]{2,1,0:T(8,128)}, u32[]{:S(2)}) copy-start(f32[4,512,256]{2,1,0:T(8,128)} %gate_hbm.1) | copy-start | bytes 6291460
  3.9 1.2 %copy-start.1 = (bf16[256,2048]{1,0:T(8,128)(2,1)S(1)}, bf16[256,2048]{1,0:T(8,128)(2,1)}, u32[]{:S(2)}) copy-start(bf16[256,2048]{1,0:T(8,128)(2,1)} %tok_hbm.1) | copy-start | bytes 3145732
  5.1 0.7 copy-start.2

commit v2 on v1

--- a/solution.py
+++ b/solution.py
@@ -9,6 +9,8 @@
 
 MESH = pl.DeviceIdType.MESH
 CHUNKS = 2
+PIECES = 4
+HALVES = 2
 
 
 def routed(tokens, norm_gain, gate_master, up_master, chosen, affinity):
@@ -127,17 +129,24 @@
     pl.semaphore_signal(barrier, 1, device_id={"tp": xq}, device_id_type=MESH)
     pl.semaphore_wait(barrier, n + 2)
 
-    def tz(s, step):
-        return remote(tok.at[s, t], tok.at[s, t], ss_tz.at[s, (step + 1) // 2], rs_tok.at[s, t], fs=z + step)
-
-    def tx(s):
-        return remote(tok.at[s, t], tok.at[s, t], ss_tx.at[s], rs_tok.at[s, t], tp=xq)
-
-    def tm(s, q, i):
-        return remote(tok.at[s, q], tok.at[s, q], ss_tm.at[s, i], rs_tok.at[s, q], tp=mate)
-
-    def tok_wait(s, q):
-        remote(tok.at[s, q], tok.at[s, q], ss_tx.at[s], rs_tok.at[s, q], tp=mate).wait_recv()
+    def block(s, q, h):
+        return tok.at[s, q, pl.ds(h * (rows // HALVES), rows // HALVES)]
+
+    def tz(s, step, h):
+        ref = block(s, t, h)
+        return remote(ref, ref, ss_tz.at[s, (step + 1) // 2, h], rs_tok.at[s, t, h], fs=z + step)
+
+    def tx(s, h):
+        ref = block(s, t, h)
+        return remote(ref, ref, ss_tx.at[s, h], rs_tok.at[s, t, h], tp=xq)
+
+    def tm(s, q, i, h):
+        ref = block(s, q, h)
+        return remote(ref, ref, ss_tm.at[s, i, h], rs_tok.at[s, q, h], tp=mate)
+
+    def tok_wait(s, q, h):
+        ref = block(s, q, h)
+        remote(ref, ref, ss_tx.at[s, h], rs_tok.at[s, q, h], tp=mate).wait_recv()
 
     def sides(d, fn):
         for sign in (1, -1):
@@ -148,7 +157,8 @@
                 fn(s, sign)
 
     tok_load(t).wait()
-    sides(1, lambda s, sign: tz(z, sign).start())
+    for h in range(HALVES):
+        sides(1, lambda s, sign: tz(z, sign, h).start())
 
     gcol = jnp.transpose(jnp.broadcast_to(gain_ref[...], (128, depth)))
     gcol = jnp.concatenate([gcol] * (fc // 128), axis=1) if fc > 128 else gcol
@@ -161,16 +171,22 @@
     def lanes(m):
         return pl.ds(pl.multiple_of(m * fc, fc), fc)
 
-    def wcopy(c, to):
-        return remote(wsend.at[to, c], W.at[z, c, :, lanes(g)], ss_w.at[c, to], rs_w.at[g, c, z], fs=to)
+    def part(p):
+        return pl.ds(p * (depth // PIECES), depth // PIECES)
+
+    def wcopy(c, p, to):
+        src, dst = wsend.at[to, c, part(p)], W.at[z, c, part(p), lanes(g)]
+        return remote(src, dst, ss_w.at[c, p, to], rs_w.at[g, c, p, z], fs=to)
 
     def send_weights(c):
-        for d in range(n - 1, 0, -1):
-            sides(d, lambda s, sign: wcopy(c, s).start())
+        for p in range(PIECES):
+            for d in range(n - 1, 0, -1):
+                sides(d, lambda s, sign: wcopy(c, p, s).start())
 
     for d in range(n - 1, 0, -1):
         sides(d, fold)
-    send_weights(0)
+    at_end = (z == 0) | (z == n - 1)
+
 
     def out_copy(m, c, s):
         ref = (gate_out, up_out)[m]
@@ -185,36 +201,48 @@
         for c in range(CHUNKS):
             W[z, c, :, m * fc : (m + 1) * fc] = (own[m, :, c * fc : (c + 1) * fc] * gcol).astype(jnp.bfloat16)
 
-    def arrive(s, sign):
-        tok_wait(s, t)
-        nxt = z - sign
-
-        @pl.when((nxt >= 0) & (nxt < n))
-        def _():
-            tz(s, -sign).start()
-
-        tx(s).start()
-        tm(s, t, 0).start()
+    def arrive_all(d):
+        for h in range(HALVES):
+
+            def arrive(s, sign):
+                tok_wait(s, t, h)
+                nxt = z - sign
+
+                @pl.when((nxt >= 0) & (nxt < n))
+                def _():
+                    tz(s, -sign, h).start()
+
+                tx(s, h).start()
+                tm(s, t, 0, h).start()
+
+            sides(d, arrive)
 
     def xrelay(s, sign):
-        tok_wait(s, xq)
-        tm(s, xq, 1).start()
-
-    def ycopy(c, s):
-        return remote(W.at[s, c, :, lanes(g)], W.at[s, c, :, lanes(g)], ss_y.at[c, s], rs_w.at[g, c, s], grp=1 - g)
+        for h in range(HALVES):
+            tok_wait(s, xq, h)
+            tm(s, xq, 1, h).start()
+
+    def ycopy(c, p, s):
+        ref = W.at[s, c, part(p), lanes(g)]
+        return remote(ref, ref, ss_y.at[c, p, s], rs_w.at[g, c, p, s], grp=1 - g)
 
     def yforward(c):
-        def one(s, sign):
-            remote(wsend.at[s, c], W.at[s, c, :, lanes(g)], ss_w.at[c, s], rs_w.at[g, c, s], fs=s).wait_recv()
-            ycopy(c, s).start()
-
-        for d in range(1, n):
-            sides(d, one)
+        for p in range(PIECES):
+
+            def one(s, sign):
+                src, dst = wsend.at[s, c, part(p)], W.at[s, c, part(p), lanes(g)]
+                remote(src, dst, ss_w.at[c, p, s], rs_w.at[g, c, p, s], fs=s).wait_recv()
+                ycopy(c, p, s).start()
+
+            for d in range(n - 1, 0, -1):
+                sides(d, one)
 
     def ywait(c):
         def one(s, sign):
             o = 1 - g
-            remote(W.at[s, c, :, lanes(o)], W.at[s, c, :, lanes(o)], ss_y.at[c, s], rs_w.at[o, c, s], grp=o).wait_recv()
+            for p in range(PIECES):
+                ref = W.at[s, c, part(p), lanes(o)]
+                remote(ref, ref, ss_y.at[c, p, s], rs_w.at[o, c, p, s], grp=o).wait_recv()
 
         for d in range(1, n):
             sides(d, one)
@@ -226,10 +254,12 @@
         return remote(hs.at[to, c], hr.at[z, c], ss_h.at[c, to], rs_h.at[c, z], fs=to)
 
     def sumsq(s):
-        total = jnp.zeros((rows, 1), jnp.float32)
+        part = jnp.zeros((rows, 128), jnp.float32)
         for q in range(nt):
-            x = tok[s, q].astype(jnp.float32)
-            total = total + jnp.sum(x * x, axis=-1, keepdims=True)
+            for i in range(depth // 128):
+                x = tok[s, q, :, i * 128 : (i + 1) * 128].astype(jnp.float32)
+                part = part + x * x
+        total = jnp.sum(part, axis=-1, keepdims=True)
         scale[s] = jnp.broadcast_to(lax.rsqrt(total / width + 1e-06), (rows, fc))
 
     def compute(c):
@@ -255,14 +285,16 @@
 
         lax.fori_loop(0, n, body, 0)
 
-    sides(1, arrive)
-    sides(2, arrive)
+    arrive_all(1)
+
+    arrive_all(2)
+    send_weights(0)
+    sides(1, xrelay)
+    for d in range(3, n):
+        arrive_all(d)
     for c in range(1, CHUNKS):
         send_weights(c)
-    sides(1, xrelay)
     yforward(0)
-    for d in range(3, n):
-        sides(d, arrive)
     for d in range(2, n):
         sides(d, xrelay)
     for off in range(1, nt):
@@ -270,50 +302,60 @@
     sumsq(z)
 
     def rest(s, sign):
-        tok_wait(s, mate)
-        tok_wait(s, xmate)
+        for h in range(HALVES):
+            tok_wait(s, mate, h)
+            tok_wait(s, xmate, h)
         sumsq(s)
 
     for d in range(1, n):
         sides(d, rest)
-    ywait(0)
-    compute(0)
     for c in range(1, CHUNKS):
         yforward(c)
+    for c in range(CHUNKS):
         ywait(c)
         compute(c)
 
     aff = aff_ref[...]
-    share = aff / jnp.sum(aff, axis=-1, keepdims=True)
-    top = aff.shape[1]
+    share = aff / jnp.sum(aff, axis=0, keepdims=True)
+    top = aff.shape[0]
+
+    def column(row):
+        col = jnp.transpose(jnp.broadcast_to(row, (128, rows)))
+        return jnp.concatenate([col] * (fc // 128), axis=1) if fc > 128 else col
+
+    shares = [column(share[k : k + 1, :]) for k in range(top)]
+    names = [column(chosen_ref[k : k + 1, :].astype(jnp.float32)) for k in range(top)]
     for c in range(CHUNKS):
         for off in range(1, n):
             s = lax.rem(z + off, n)
             remote(hs.at[s, c], hr.at[s, c], ss_h.at[c, s], rs_h.at[c, s], fs=s).wait_recv()
         for k in range(top):
-            ch = jnp.broadcast_to(chosen_ref[:, k : k + 1], (rows, fc))
             picked = jnp.zeros((rows, fc), jnp.float32)
             for e in range(n):
-                picked = jnp.where(ch == e, hr[e, c].astype(jnp.float32), picked)
+                picked = jnp.where(names[k] == e, hr[e, c].astype(jnp.float32), picked)
             hid_out[:, k * fcols + c * fc : k * fcols + (c + 1) * fc] = (
-                picked * share[:, k : k + 1]
+                picked * shares[k]
             ).astype(jnp.bfloat16)
 
-    sides(1, lambda s, sign: tz(z, sign).wait_send())
+    for h in range(HALVES):
+        sides(1, lambda s, sign: tz(z, sign, h).wait_send())
 
     def drain(s, sign):
         nxt = z - sign
 
-        @pl.when((nxt >= 0) & (nxt < n))
-        def _():
-            tz(s, -sign).wait_send()
-
-        tx(s).wait_send()
-        tm(s, t, 0).wait_send()
-        tm(s, xq, 1).wait_send()
+        for h in range(HALVES):
+
+            @pl.when((nxt >= 0) & (nxt < n))
+            def _():
+                tz(s, -sign, h).wait_send()
+
+            tx(s, h).wait_send()
+            tm(s, t, 0, h).wait_send()
+            tm(s, xq, 1, h).wait_send()
         for c in range(CHUNKS):
-            wcopy(c, s).wait_send()
-            ycopy(c, s).wait_send()
+            for p in range(PIECES):
+                wcopy(c, p, s).wait_send()
+                ycopy(c, p, s).wait_send()
             hcopy(c, s).wait_send()
 
     for d in range(1, n):
@@ -333,6 +375,7 @@
     bf, f32 = jnp.bfloat16, jnp.float32
     dma = pltpu.SemaphoreType.DMA
     any_spec = pl.BlockSpec(memory_space=pl.ANY)
+    hbm = pl.BlockSpec(memory_space=pltpu.HBM)
     vmem = pl.BlockSpec(memory_space=pltpu.VMEM)
     gate, up, hid = pl.pallas_call(
         functools.partial(dense_kernel, n, nt, width),
@@ -341,7 +384,7 @@
             jax.ShapeDtypeStruct((1, width, fcols), bf),
             jax.ShapeDtypeStruct((rows, top * fcols), bf),
         ),
-        in_specs=[any_spec, vmem, any_spec, any_spec, vmem, vmem],
+        in_specs=[hbm, vmem, hbm, hbm, vmem, vmem],
         out_specs=(any_spec, any_spec, vmem),
         scratch_shapes=[
             pltpu.VMEM((n, nt, rows, depth), bf),
@@ -356,20 +399,20 @@
             dma((n,)),
             dma((2,)),
             dma((2, CHUNKS, n)),
-            dma((n, 2)),
-            dma((n,)),
-            dma((n, 2)),
-            dma((n, nt)),
-            dma((CHUNKS, n)),
-            dma((2, CHUNKS, n)),
-            dma((CHUNKS, n)),
+            dma((n, 2, HALVES)),
+            dma((n, HALVES)),
+            dma((n, 2, HALVES)),
+            dma((n, nt, HALVES)),
+            dma((CHUNKS, PIECES, n)),
+            dma((2, CHUNKS, PIECES, n)),
+            dma((CHUNKS, PIECES, n)),
             dma((CHUNKS, n)),
             dma((CHUNKS, n)),
         ],
         compiler_params=pltpu.CompilerParams(
-            collective_id=0, has_side_effects=True, vmem_limit_bytes=48 * 1024 * 1024
+            collective_id=0, has_side_effects=True, vmem_limit_bytes=50 * 1024 * 1024
         ),
-    )(tokens, norm_gain.reshape(1, depth), gate_master, up_master, chosen, affinity)
+    )(tokens, norm_gain.reshape(1, depth), gate_master, up_master, chosen.T, affinity.T)
     return gate, up, hid.reshape(rows, top, fcols)
 
 

time: 79.6 us -> 63.1 us (0.79)
  Pallas kernels: 70.9 us -> 56.2 us
  local copies, waits for them, and re-layouts: 7.82 us -> 5.97 us
    pallas_call x1, Pallas kernels: 70.9 us -> 56.2 us  [dense(): pl.pallas_call(functools.partial(dense_kernel, n, nt, width), out_shape=(...]
    unnamed x10, local copies, waits for them, and re-layouts: 7.06 us -> 5.2 us
where the time goes in v2:
time: 63.1 us; the launch traced here: 62.8 us
  Pallas kernels  56.2 us (89%)
  local copies, waits for them, and re-layouts  5.97 us (9%)
  between operations  0.65 us (1%)
    pallas_call x1, Pallas kernels, dense(): pl.pallas_call(functools.partial(dense_kernel, n, nt, width), out_shape=(...  56.2 us
    unnamed x10, local copies, waits for them, and re-layouts  5.2 us

profile of v2, /device:TPU:0, one launch (start us, length us, event | category | flops | bytes accessed | tf_op | source)
XLA Modules:
  0.0 62.8 jit_solution(18273558773554127587)
XLA Ops:
  0.6 0.0 copy-start
  0.6 1.2 %copy-done = bf16[256,2048]{1,0:T(8,128)(2,1)S(1)} copy-done((bf16[256,2048]{1,0:T(8,128)(2,1)S(1)}, bf16[256,2048]{1,0:T(8,128)(2,1)}, u32[]{:S(2)}) %copy-start) | copy-done | bytes 1048600
  1.9 0.0 copy-start.1
  1.9 0.7 %copy-done.1 = f32[512]{0:T(512)S(1)} copy-done((f32[512]{0:T(512)S(1)}, f32[512]{0:T(512)}, u32[]{:S(2)}) %copy-start.1) | copy-done | bytes 2072
  2.5 0.0 copy-start.2
  2.5 0.7 %copy-done.2 = s32[256,2]{0,1:T(2,128)S(1)} copy-done((s32[256,2]{0,1:T(2,128)S(1)}, s32[256,2]{0,1:T(2,128)}, u32[]{:S(2)}) %copy-start.2) | copy-done | bytes 2072
  3.2 0.0 copy-start.3
  3.2 0.7 %copy-done.3 = f32[256,2]{0,1:T(2,128)S(1)} copy-done((f32[256,2]{0,1:T(2,128)S(1)}, f32[256,2]{0,1:T(2,128)}, u32[]{:S(2)}) %copy-start.3) | copy-done | bytes 2072
  3.9 56.2 %shard_map.85 = (bf16[1,2048,256]{2,1,0:T(8,128)(2,1)S(1)}, bf16[1,2048,256]{2,1,0:T(8,128)(2,1)S(1)}, bf16[256,512]{1,0:T(8,128)(2,1)S(1)}) custom-call(bf16[256,2048]{1,0:T(8,128)(2,1)S(1)} %copy-done, f32[1,512]{1,0:T(1,128)S(1)} %bitcast.3, f32[4,512,256]{2,1,0:T(8,128)} %gate_hbm.1, f32[4,512,256]{2,1,0:T(8,128)} %up_hbm.1, s32[2,256]{1,0:T(2,128)S(1)} %bitcast.4, ...), custom_call_target="tpu_custom_call" | custom-call | tf_op jit(solution)/shard_map/pallas_call | solution.py:380
  60.1 0.8 %reshape.13 = bf16[256,2,256]{2,1,0:T(2,128)(2,1)} reshape(bf16[256,512]{1,0:T(8,128)(2,1)S(1)} %get-tuple-element.8) | data formatting | bytes 524288 | tf_op jit(solution)/shard_map/reshape | solution.py:416
  60.9 1.0 %copy.11 = bf16[1,2048,256]{2,1,0:T(8,128)(2,1)} copy(bf16[1,2048,256]{2,1,0:T(8,128)(2,1)S(1)} %get-tuple-element.12) | data formatting | bytes 2097152
  61.9 1.0 %copy.12 = bf16[1,2048,256]{2,1,0:T(8,128)(2,1)} copy(bf16[1,2048,256]{2,1,0:T(8,128)(2,1)S(1)} %get-tuple-element.13) | data formatting | bytes 2097152
Async XLA Ops:
  0.6 1.2 %copy-start = (bf16[256,2048]{1,0:T(8,128)(2,1)S(1)}, bf16[256,2048]{1,0:T(8,128)(2,1)}, u32[]{:S(2)}) copy-start(bf16[256,2048]{1,0:T(8,128)(2,1)} %tok_hbm.1) | copy-start | bytes 3145732
  1.9 0.7 %copy-start.1 = (f32[512]{0:T(512)S(1)}, f32[512]{0:T(512)}, u32[]{:S(2)}) copy-start(f32[512]{0:T(512)} %param.7) | copy-start | bytes 6148
  2.5 0.7 %copy-start.2 = (s32[256,2]{0,1:T(2,128)S(1)}, s32[256,2]{0,1:T(2,128)}, u32[]{:S(2)}) copy-start(s32[256,2]{0,1:T(2,128)} %param.10) | copy-start | bytes 6148
  3.2 0.7 %copy-start.3 = (f32[256,2]{0,1:T(2,128)S(1)}, f32[256,2]{0,1:T(2,128)}, u32[]{:S(2)}) copy-start(f32[256,2]{0,1:T(2,128)} %param.11) | copy-start | bytes 6148

commit v3 on v2

--- a/solution.py
+++ b/solution.py
@@ -410,7 +410,7 @@
             dma((CHUNKS, n)),
         ],
         compiler_params=pltpu.CompilerParams(
-            collective_id=0, has_side_effects=True, vmem_limit_bytes=50 * 1024 * 1024
+            collective_id=0, has_side_effects=True, vmem_limit_bytes=51 * 1024 * 1024
         ),
     )(tokens, norm_gain.reshape(1, depth), gate_master, up_master, chosen.T, affinity.T)
     return gate, up, hid.reshape(rows, top, fcols)

time: 63.1 us -> 61.7 us (0.978)
  local copies, waits for them, and re-layouts: 5.97 us -> 4.74 us
    unnamed x10 -> x8, local copies, waits for them, and re-layouts: 5.2 us -> 3.98 us
where the time goes in v3:
time: 61.7 us; the launch traced here: 61.5 us
  Pallas kernels  56.1 us (91%)
  local copies, waits for them, and re-layouts  4.74 us (8%)
  between operations  0.65 us (1%)
    pallas_call x1, Pallas kernels, dense(): pl.pallas_call(functools.partial(dense_kernel, n, nt, width), out_shape=(...  56.1 us
    unnamed x8, local copies, waits for them, and re-layouts  3.98 us

profile of v3, /device:TPU:0, one launch (start us, length us, event | category | flops | bytes accessed | tf_op | source)
XLA Modules:
  0.0 61.5 jit_solution(10880582541157975687)
XLA Ops:
  0.6 0.0 copy-start
  0.6 0.7 %copy-done = f32[512]{0:T(512)S(1)} copy-done((f32[512]{0:T(512)S(1)}, f32[512]{0:T(512)}, u32[]{:S(2)}) %copy-start) | copy-done | bytes 2072
  1.3 0.0 copy-start.1
  1.3 0.7 %copy-done.1 = s32[256,2]{0,1:T(2,128)S(1)} copy-done((s32[256,2]{0,1:T(2,128)S(1)}, s32[256,2]{0,1:T(2,128)}, u32[]{:S(2)}) %copy-start.1) | copy-done | bytes 2072
  2.0 0.0 copy-start.2
  2.0 0.7 %copy-done.2 = f32[256,2]{0,1:T(2,128)S(1)} copy-done((f32[256,2]{0,1:T(2,128)S(1)}, f32[256,2]{0,1:T(2,128)}, u32[]{:S(2)}) %copy-start.2) | copy-done | bytes 2072
  2.7 56.1 %shard_map.85 = (bf16[1,2048,256]{2,1,0:T(8,128)(2,1)S(1)}, bf16[1,2048,256]{2,1,0:T(8,128)(2,1)S(1)}, bf16[256,512]{1,0:T(8,128)(2,1)S(1)}) custom-call(bf16[256,2048]{1,0:T(8,128)(2,1)} %tok_hbm.1, f32[1,512]{1,0:T(1,128)S(1)} %bitcast.3, f32[4,512,256]{2,1,0:T(8,128)} %gate_hbm.1, f32[4,512,256]{2,1,0:T(8,128)} %up_hbm.1, s32[2,256]{1,0:T(2,128)S(1)} %bitcast.4, ...), custom_call_target="tpu_custom_call" | custom-call | tf_op jit(solution)/shard_map/pallas_call | solution.py:380
  58.8 0.8 %reshape.13 = bf16[256,2,256]{2,1,0:T(2,128)(2,1)} reshape(bf16[256,512]{1,0:T(8,128)(2,1)S(1)} %get-tuple-element.8) | data formatting | bytes 524288 | tf_op jit(solution)/shard_map/reshape | solution.py:416
  59.5 1.0 %copy.11 = bf16[1,2048,256]{2,1,0:T(8,128)(2,1)} copy(bf16[1,2048,256]{2,1,0:T(8,128)(2,1)S(1)} %get-tuple-element.12) | data formatting | bytes 2097152
  60.5 1.0 %copy.12 = bf16[1,2048,256]{2,1,0:T(8,128)(2,1)} copy(bf16[1,2048,256]{2,1,0:T(8,128)(2,1)S(1)} %get-tuple-element.13) | data formatting | bytes 2097152
Async XLA Ops:
  0.6 0.7 %copy-start = (f32[512]{0:T(512)S(1)}, f32[512]{0:T(512)}, u32[]{:S(2)}) copy-start(f32[512]{0:T(512)} %param.7) | copy-start | bytes 6148
  1.3 0.7 %copy-start.1 = (s32[256,2]{0,1:T(2,128)S(1)}, s32[256,2]{0,1:T(2,128)}, u32[]{:S(2)}) copy-start(s32[256,2]{0,1:T(2,128)} %param.10) | copy-start | bytes 6148
  2.0 0.7 %copy-start.2 = (f32[256,2]{0,1:T(2,128)S(1)}, f32[256,2]{0,1:T(2,128)}, u32[]{:S(2)}) copy-start(f32[256,2]{0,1:T(2,128)} %param.11) | copy-start | bytes 6148
